TPU v7x, 32 devices: a whole 2x2x4 slice. The times are simulated.
32 devices in a mesh: grp: 2 (over y), ep: 8 (over z, core), tp: 2 (over x).
Axes of the slice: x: 2, y: 2, z: 4, core: 2. Of those that a mesh axis runs over, the one named last changes fastest.
Arguments:
- tokens: bfloat16 [2048, 4096], P(('grp', 'ep'), 'tp'), parts along dimension 0, may hold values from -6 to 6
- routes: int32 [2048, 4], P(('grp', 'ep')), parts along dimension 0, may hold values from 0 to 7, all different within a row; in each aligned block of 128 rows (0 to 127, 128 to 255, ...) at most 128 rows name the same one
- route_weights: float32 [2048, 4], P(('grp', 'ep')), parts along dimension 0, may hold values from 0.1 to 1
- norm_gain: float32 [4096], replicated, may hold values from 0.1 to 1.9
- expert_gate: bfloat16 [8, 4096, 1024], P('ep', 'tp'), may hold values from -0.09375 to 0.09375
- expert_up: bfloat16 [8, 4096, 1024], P('ep', 'tp'), may hold values from -0.09375 to 0.09375
- expert_down: bfloat16 [8, 1024, 4096], P('ep', None, 'tp')
- shared_gate: bfloat16 [4096, 1024], P('tp'), may hold values from -0.09375 to 0.09375
- shared_up: bfloat16 [4096, 1024], P('tp'), may hold values from -0.09375 to 0.09375
- shared_down: bfloat16 [1024, 4096], P(None, 'tp')
- out_gain: float32 [4096], P('tp'), may hold values from 0.1 to 1.9
Outputs:
- layer_out: bfloat16 [2048, 4096], P(('grp', 'ep'), 'tp'), parts along dimension 0
There are 2 independent parts, one for each index of `grp`. A program takes and returns all parts, laid end to end along the dimension named above; an argument that names none is the same for every part. Nothing has to cross between parts.
Inputs may be any that keep to these rules, and one draw needn't show every extreme that they name: `routes`: each row names 4 different experts; among the rows of one index of ep no expert is named more than 128 times, and in some such block some expert is named exactly 128 times.
All inputs are finite; a program needn't handle non-finite values.
Results may differ from a plain program's by a relative error of at most 0.023.
Values may be sent and summed in bfloat16 or wider, within the bound.
A program may use at most 64 MiB of HBM per device.

v0:
```python
import jax
import jax.numpy as jnp
from jax import lax
from jax.sharding import PartitionSpec as P

epsilon = 1e-06


def local_product(source, matrix):
    return jnp.dot(source, matrix, preferred_element_type=jnp.float32)


def per_device(
    tokens,
    routes,
    route_weights,
    norm_gain,
    expert_gate,
    expert_up,
    expert_down,
    shared_gate,
    shared_up,
    shared_down,
    out_gain,
):
    block_width = tokens.shape[1]
    full_width = block_width * lax.axis_size("tp")
    width_index = lax.axis_index("tp")
    full_rows = lax.all_gather(tokens, "tp", axis=1, tiled=True)
    full_float = full_rows.astype(jnp.float32)
    normed_full = (
        full_float
        * lax.rsqrt(jnp.mean(full_float * full_float, axis=-1, keepdims=True) + epsilon)
        * norm_gain
    ).astype(jnp.bfloat16)
    normed_block = lax.dynamic_slice_in_dim(normed_full, width_index * block_width, block_width, 1)
    gate_matrix = expert_gate[0]
    up_matrix = expert_up[0]
    down_matrix = expert_down[0]
    experts = lax.axis_size("ep")
    choose = (routes[:, :, None] == jnp.arange(experts, dtype=jnp.int32)[None, None, :]).astype(
        jnp.float32
    )
    weight_table = jnp.sum(route_weights[:, :, None] * choose, axis=1)
    expert_input = lax.all_gather(normed_block, "ep", axis=0, tiled=True)
    table_all = lax.all_gather(weight_table, "ep", axis=0, tiled=True)
    summed = (
        lax.psum(local_product(expert_input, gate_matrix).astype(jnp.bfloat16), "tp").astype(
            jnp.float32
        ),
        lax.psum(local_product(expert_input, up_matrix).astype(jnp.bfloat16), "tp").astype(
            jnp.float32
        ),
        lax.psum(local_product(normed_block, shared_gate).astype(jnp.bfloat16), "tp").astype(
            jnp.float32
        ),
        lax.psum(local_product(normed_block, shared_up).astype(jnp.bfloat16), "tp").astype(
            jnp.float32
        ),
    )
    routed_hidden = (jax.nn.silu(summed[0]) * summed[1]).astype(jnp.bfloat16)
    shared_hidden = (jax.nn.silu(summed[2]) * summed[3]).astype(jnp.bfloat16)
    expert_rows = local_product(routed_hidden, down_matrix).astype(jnp.bfloat16)
    shared_out = local_product(shared_hidden, shared_down)
    own_expert = lax.axis_index("ep")
    column = lax.dynamic_slice_in_dim(table_all, own_expert, 1, 1)
    routed = lax.psum_scatter(
        (column * expert_rows.astype(jnp.float32)).astype(jnp.bfloat16),
        "ep",
        scatter_dimension=0,
        tiled=True,
    ).astype(jnp.float32)
    mixture = routed + shared_out
    square_sum = lax.psum(jnp.sum(mixture * mixture, axis=-1, keepdims=True), "tp")
    scale = lax.rsqrt(square_sum / full_width + epsilon)
    return (mixture * scale * out_gain).astype(jnp.bfloat16)


def solution(mesh):
    return jax.shard_map(
        per_device,
        mesh=mesh,
        in_specs=(
            P(("grp", "ep"), "tp"),
            P(("grp", "ep"), None),
            P(("grp", "ep"), None),
            P(),
            P("ep", "tp", None),
            P("ep", "tp", None),
            P("ep", None, "tp"),
            P("tp", None),
            P("tp", None),
            P(None, "tp"),
            P("tp"),
        ),
        out_specs=P(("grp", "ep"), "tp"),
        check_vma=False,
    )
```

profile of v0, /device:TPU:9, one launch (start us, length us, event | category | flops | bytes accessed | tf_op | source)
XLA Modules:
  0.0 289.5 jit_solution(16838798850096647116)
XLA Ops:
  6.5 0.0 all-gather.3.cloned.1.call-start
  6.5 0.7 all-gather.3.cloned.1.call-update
  7.3 0.0 all-gather.5.cloned.1.call-start
  7.3 0.0 dynamic-slice-start
  7.3 23.9 %all-gather.3.cloned.1.call-done = bf16[128,4096]{1,0:T(8,128)(2,1)} async-done(((bf16[128,2048]{1,0:T(8,128)(2,1)}), bf16[128,4096]{1,0:T(8,128)(2,1)}) %all-gather.3.cloned.1.call-update) | async-done | bytes 1048592 | tf_op jit(solution)/shard_map/all_gather | solution.py:29
  31.2 1.5 multiply_reduce_fusion
  32.7 1.4 convert_element_type.52
  34.1 0.0 dynamic-slice-done
  34.2 1.0 fusion.22
  35.1 0.0 copy-start
  35.1 0.0 all-gather.5.cloned.1.call-update
  35.1 0.0 all-reduce.3.cloned.1.call-start
  35.2 0.0 copy-start.1
  35.2 3.9 %convolution_convert_fusion = bf16[128,1024]{1,0:T(8,128)(2,1)} fusion(bf16[128,2048]{1,0:T(8,128)(2,1)} %fusion.22, bf16[2048,1024]{1,0:T(8,128)(2,1)} %param.19), kind=kOutput, calls=%fused_computation.19 | convolution fusion | flops 537001984 | bytes 4980736 | tf_op jit(solution)/shard_map/dot_general | solution.py:10
  39.1 0.0 copy-done
  39.1 0.0 copy-done.1
  39.1 1.5 convolution_convert_fusion.1
  40.6 40.9 %all-gather.5.cloned.1.call-done = bf16[1024,2048]{1,0:T(8,128)(2,1)} async-done(((bf16[128,2048]{1,0:T(8,128)(2,1)}), bf16[1024,2048]{1,0:T(8,128)(2,1)}) %all-gather.5.cloned.1.call-update) | async-done | bytes 4194320 | tf_op jit(solution)/shard_map/all_gather | solution.py:45
  81.5 0.0 copy-start.5
  81.5 0.0 copy-start.6
  81.5 9.5 %fusion.15 = bf16[1024,1024]{1,0:T(8,128)(2,1)} fusion(bf16[1024,2048]{1,0:T(8,128)(2,1)} %all-gather.5.cloned.1.call-done, bf16[1,2048,1024]{2,1,0:T(8,128)(2,1)} %param.15), kind=kOutput, calls=%fused_computation.17 | convolution fusion | flops 4296015872 | bytes 10485760 | tf_op jit(solution)/shard_map/dot_general | solution.py:10
  91.0 0.0 copy-done.5
  91.0 0.0 copy-done.6
  91.0 5.7 %fusion.18 = bf16[1024,1024]{1,0:T(8,128)(2,1)} fusion(bf16[1024,2048]{1,0:T(8,128)(2,1)S(1)} %copy-done.6, bf16[1,2048,1024]{2,1,0:T(8,128)(2,1)S(1)} %copy-done.5), kind=kOutput, calls=%fused_computation.18 | convolution fusion | flops 4296015872 | bytes 10485760 | tf_op jit(solution)/shard_map/dot_general | solution.py:10
  96.7 0.0 copy-start.3
  96.7 0.0 copy-start.4
  96.7 0.0 all-reduce.3.cloned.1.call-update
  96.7 0.0 reduce-scatter.2.cloned.1.call-start
  96.8 0.6 copy-done.3
  97.4 0.0 copy-done.4
  97.4 13.5 %all_gather.9 = f32[1024,8]{0,1:T(8,128)S(1)} all-gather(f32[128,8]{0,1:T(8,128)S(1)} %select_reduce_fusion), channel_id=1, replica_groups=mesh['grp'=2,'ep'=8,'tp'=2] {'ep'}, dimensions={0}, use_global_device_ids=true | all-gather | bytes 36864 | tf_op jit(solution)/shard_map/all_gather | solution.py:46
  110.9 104.7 %all-reduce.3.cloned.1.call-done = (bf16[1024,1024]{1,0:T(8,128)(2,1)}, bf16[1024,1024]{1,0:T(8,128)(2,1)}, bf16[128,1024]{1,0:T(8,128)(2,1)}, bf16[128,1024]{1,0:T(8,128)(2,1)}) async-done(((bf16[1024,1024]{1,0:T(8,128)(2,1)}, bf16[1024,1024]{1,0:T(8,128)(2,1)}, bf16[128,1024]{1,0:T(8,128)(2,1)}, bf16[128,1024]{1,0:T(8,128)(2,1)}), (bf16[1024,1024]{1,0:T(8,128)(2,1)}, bf16[1024,1024]{1,0:T(8,128)(2,1)}, ...) | async-done | bytes 4718608 | tf_op jit(solution)/shard_map/psum | solution.py:51
  215.6 10.3 %multiply_convert_fusion = bf16[1024,2048]{1,0:T(8,128)(2,1)} fusion(f32[1024]{0:T(1024)S(1)} %bitcast.26, bf16[1,1024,2048]{2,1,0:T(8,128)(2,1)} %param.17, bf16[1024,1024]{1,0:T(8,128)(2,1)} %get-tuple-element.5, bf16[1024,1024]{1,0:T(8,128)(2,1)} %get-tuple-element.6), kind=kOutput, calls=%fused_computation | convolution fusion | flops 4311744512 | bytes 12587008 | tf_op jit(solution)/shard_map/dot_general | solution.py:10
  226.0 0.0 copy-start.7
  226.0 0.0 copy-start.8
  226.0 0.0 reduce-scatter.2.cloned.1.call-update
  226.0 0.0 copy-start.2
  226.0 49.0 %reduce-scatter.2.cloned.1.call-done = bf16[128,2048]{1,0:T(8,128)(2,1)} async-done(((bf16[1024,2048]{1,0:T(8,128)(2,1)}), bf16[128,2048]{1,0:T(8,128)(2,1)}) %reduce-scatter.2.cloned.1.call-update) | async-done | bytes 524304 | tf_op jit(solution)/shard_map/reduce_scatter | solution.py:67
  275.0 0.0 copy-done.7
  275.0 0.0 copy-done.8
  275.0 3.2 %multiply_reduce_fusion.1 = (f32[128]{0:T(128)S(1)}, f32[128,2048]{1,0:T(8,128)S(1)}) fusion(bf16[1024,2048]{1,0:T(8,128)(2,1)} %param.20, bf16[128,1024]{1,0:T(8,128)(2,1)S(1)} %copy-done.7, bf16[128,1024]{1,0:T(8,128)(2,1)S(1)} %copy-done.8, bf16[128,2048]{1,0:T(8,128)(2,1)} %reduce-scatter.2.cloned.1.call-done), kind=kOutput, calls=%fused_computation.25 | convolution fusion | flops 538967936 | bytes 6291968 | tf_op jit(solution)/shard_map/dot_general | solution.py:10
  278.2 3.8 %psum.39 = f32[128,1]{0,1:T(1,128)S(1)} all-reduce(f32[128,1]{0,1:T(1,128)S(1)} %bitcast.27), channel_id=1, replica_groups=mesh['grp'=2,'ep'=8,'tp'=2] {'tp'}, use_global_device_ids=true, to_apply=%region_8.9 | all-reduce | flops 128 | bytes 1024 | tf_op jit(solution)/shard_map/psum | solution.py:74
  282.0 0.0 copy-done.2
  282.0 1.0 multiply_convert_fusion.1
  (4 shorter events, 0.0 us)
Async XLA Ops:
  6.5 24.6 %all-gather.3.cloned.1.call-start = ((), (), s32[]{:S(2)}) async-start(), calls=%async_computation.1 | async-start | bytes 1572864 | tf_op jit(solution)/shard_map/all_gather | solution.py:29
  7.3 74.2 %all-gather.5.cloned.1.call-start = ((), (), s32[]{:S(2)}) async-start(), calls=%async_computation.2 | async-start | bytes 4718592 | tf_op jit(solution)/shard_map/all_gather | solution.py:45
  7.3 26.8 %dynamic-slice-start = ((f32[4096]{0:T(1024)}, s32[]{:T(128)}), f32[2048]{0:T(1024)S(1)}, s32[]{:S(2)}) async-start(f32[4096]{0:T(1024)} %param.14, s32[]{:T(128)} %select_n.7), calls=%async_computation.5 | async-start | bytes 16896 | tf_op jit(solution)/shard_map/dynamic_slice | solution.py:36
  35.1 4.0 %copy-start = (bf16[128,2048]{1,0:T(8,128)(2,1)S(1)}, bf16[128,2048]{1,0:T(8,128)(2,1)}, u32[]{:S(2)}) copy-start(bf16[128,2048]{1,0:T(8,128)(2,1)} %fusion.22) | copy-start | bytes 1572868
  35.1 180.5 %all-reduce.3.cloned.1.call-start = ((), (), s32[]{:S(2)}) async-start(), calls=%async_computation.4 | async-start | bytes 9437184 | tf_op jit(solution)/shard_map/psum | solution.py:51
  35.2 3.9 %copy-start.1 = (bf16[2048,1024]{1,0:T(8,128)(2,1)S(1)}, bf16[2048,1024]{1,0:T(8,128)(2,1)}, u32[]{:S(2)}) copy-start(bf16[2048,1024]{1,0:T(8,128)(2,1)} %param.18) | copy-start | bytes 12582916
  81.5 9.5 %copy-start.5 = (bf16[1,2048,1024]{2,1,0:T(8,128)(2,1)S(1)}, bf16[1,2048,1024]{2,1,0:T(8,128)(2,1)}, u32[]{:S(2)}) copy-start(bf16[1,2048,1024]{2,1,0:T(8,128)(2,1)} %param.16) | copy-start | bytes 12582916
  81.5 9.5 %copy-start.6 = (bf16[1024,2048]{1,0:T(8,128)(2,1)S(1)}, bf16[1024,2048]{1,0:T(8,128)(2,1)}, u32[]{:S(2)}) copy-start(bf16[1024,2048]{1,0:T(8,128)(2,1)} %all-gather.5.cloned.1.call-done) | copy-start | bytes 12582916
  96.7 0.7 copy-start.3
  96.7 0.7 copy-start.4
  96.7 178.3 %reduce-scatter.2.cloned.1.call-start = ((), (), s32[]{:S(2)}) async-start(), calls=%async_computation.3 | async-start | bytes 4718592 | tf_op jit(solution)/shard_map/reduce_scatter | solution.py:67
  226.0 49.0 %copy-start.7 = (bf16[128,1024]{1,0:T(8,128)(2,1)S(1)}, bf16[128,1024]{1,0:T(8,128)(2,1)}, u32[]{:S(2)}) copy-start(bf16[128,1024]{1,0:T(8,128)(2,1)} %get-tuple-element.7) | copy-start | bytes 786436
  226.0 49.0 %copy-start.8 = (bf16[128,1024]{1,0:T(8,128)(2,1)S(1)}, bf16[128,1024]{1,0:T(8,128)(2,1)}, u32[]{:S(2)}) copy-start(bf16[128,1024]{1,0:T(8,128)(2,1)} %get-tuple-element.8) | copy-start | bytes 786436
  226.0 56.0 %copy-start.2 = (f32[2048]{0:T(1024)S(1)}, f32[2048]{0:T(1024)}, u32[]{:S(2)}) copy-start(f32[2048]{0:T(1024)} %param.21) | copy-start | bytes 24580
Sparse Core Ops, SparseCore 0:
  8.9 22.2 all-gather.2
  35.3 46.1 all-gather.4
  96.8 118.7 all-reduce.2
  226.1 48.8 reduce-scatter.1
where the time goes:
time: 294 us; the launch traced here: 289 us
  waiting for transfers between devices  219 us (74%)
  matrix products  34.1 us (12%)
  blocking collectives  17.3 us (6%)
  between operations  13.2 us (4%)
  other arithmetic  4.88 us (2%)
    psum x1, waiting for transfers between devices, per_device(): lax.psum(local_product(expert_input, up_matrix).astype(jnp.bfloat16), 'tp')  105 us
    reduce_scatter x1, waiting for transfers between devices, per_device(): lax.psum_scatter((column * expert_rows.astype(jnp.float32)).astype(jnp.bf...  49 us
    all_gather x1, waiting for transfers between devices, per_device(): expert_input = lax.all_gather(normed_block, 'ep', axis=0, tiled=True)  40.9 us
    dot_general x6, matrix products, local_product(): return jnp.dot(source, matrix, preferred_element_type=jnp.float32)  34.1 us
    all_gather x1, waiting for transfers between devices, per_device(): full_rows = lax.all_gather(tokens, 'tp', axis=1, tiled=True)  23.9 us
    all_gather x1, blocking collectives, per_device(): table_all = lax.all_gather(weight_table, 'ep', axis=0, tiled=True)  13.5 us
  transfers between devices with their start and end apart: 4, of which 4 were waited for; matrix products, arithmetic and copies ran while one was open for 2% of the time, Pallas kernels for 0%

commit v1 on v0

--- a/solution.py
+++ b/solution.py
@@ -1,9 +1,485 @@
+import functools
+
 import jax
 import jax.numpy as jnp
 from jax import lax
+from jax.experimental import pallas as pl
+from jax.experimental.pallas import tpu as pltpu
 from jax.sharding import PartitionSpec as P
 
 epsilon = 1e-06
+MESH = pl.DeviceIdType.MESH
+TABLE = 128
+
+
+def plan(chips):
+    steps = [(0, 0), None, (1, 0)]
+    for mask in range(2, chips):
+        steps += [(mask, 0), (mask, 1)]
+    steps += [(1, 1), (0, 1)]
+    relays = []
+    for distance in range(1, chips):
+        relays.append(next(i for i, s in enumerate(steps) if s is not None and s[0] >= distance))
+    return steps, relays
+
+
+def pick(index, table):
+    value = jnp.int32(table[0])
+    for position in range(1, len(table)):
+        if table[position] != table[0]:
+            value = jnp.where(index == position, jnp.int32(table[position]), value)
+    return value
+
+
+def exclusive_or(a, b, size):
+    total, unit = jnp.int32(0), 1
+    while unit < size:
+        total = total + unit * lax.rem(lax.div(a, unit) + lax.div(b, unit), 2)
+        unit *= 2
+    return total
+
+
+def fused_kernel(
+    chips,
+    tokens_ref,
+    routes_ref,
+    weights_ref,
+    norm_gain_ref,
+    gate_hbm,
+    up_hbm,
+    down_hbm,
+    shared_gate_hbm,
+    shared_up_hbm,
+    shared_down_hbm,
+    out_gain_ref,
+    out_ref,
+    gate,
+    up,
+    down,
+    held,
+    part_out,
+    part_in,
+    part_own,
+    hidden,
+    product,
+    pair_out,
+    pair_in,
+    far_out,
+    far_in,
+    mixture,
+    square_out,
+    square_in,
+    load_sem,
+    square_send,
+    square_recv,
+    gather_send,
+    gather_recv,
+    pair_gather_recv,
+    part_send,
+    part_recv,
+    hidden_send,
+    hidden_recv,
+    pair_send,
+    pair_recv,
+    far_send,
+    far_recv,
+):
+    rows, width = tokens_ref.shape
+    experts = 2 * chips
+    units = gate.shape[2]
+    half = units // 2
+    steps, relays = plan(chips)
+    count = len(steps)
+    masks = [0 if s is None else s[0] for s in steps]
+    lanes = [0 if s is None else s[1] for s in steps]
+    shared_at = steps.index(None)
+
+    ep = lax.axis_index("ep")
+    tp = lax.axis_index("tp")
+    chip, core = lax.div(ep, 2), lax.rem(ep, 2)
+    other_core = 1 - core
+    partner = {"ep": chip * 2 + other_core}
+    across = {"tp": 1 - tp}
+
+    loads = [
+        pltpu.make_async_copy(source, target, load_sem.at[i])
+        for i, (source, target) in enumerate(
+            [
+                (gate_hbm.at[0], gate.at[0]),
+                (up_hbm.at[0], up.at[0]),
+                (shared_gate_hbm, gate.at[1]),
+                (shared_up_hbm, up.at[1]),
+                (down_hbm.at[0], down.at[0]),
+                (shared_down_hbm, down.at[1]),
+            ]
+        )
+    ]
+    for load in loads:
+        load.start()
+
+    barrier = pltpu.get_barrier_semaphore()
+    for shift in range(1, chips):
+        pl.semaphore_signal(
+            barrier,
+            inc=1,
+            device_id={"ep": lax.rem(chip + shift, chips) * 2 + core},
+            device_id_type=MESH,
+        )
+    pl.semaphore_signal(barrier, inc=1, device_id=partner, device_id_type=MESH)
+    pl.semaphore_signal(barrier, inc=1, device_id=across, device_id_type=MESH)
+
+    def remote(source, target, send, recv, device):
+        return pltpu.make_async_remote_copy(
+            src_ref=source,
+            dst_ref=target,
+            send_sem=send,
+            recv_sem=recv,
+            device_id=device,
+            device_id_type=MESH,
+        )
+
+    def square_copy(which):
+        return remote(
+            square_out.at[which],
+            square_in.at[which],
+            square_send.at[which],
+            square_recv.at[which],
+            across,
+        )
+
+    def gather_copy(origin, way):
+        slot = held.at[origin * 2 + core]
+        device = ({"ep": (chip - 1) * 2 + core}, {"ep": (chip + 1) * 2 + core}, partner)[way]
+        recv = (pair_gather_recv if way == 2 else gather_recv).at[origin]
+        return remote(slot, slot, gather_send.at[origin, way], recv, device)
+
+    def pair_gather_arrival(origin):
+        slot = held.at[origin * 2 + other_core]
+        return remote(slot, slot, gather_send.at[origin, 2], pair_gather_recv.at[origin], partner)
+
+    def part_copy(k):
+        return remote(part_out.at[k], part_in.at[k], part_send.at[k], part_recv.at[k], across)
+
+    def hidden_copy(k, side):
+        return remote(
+            hidden.at[k, side], hidden.at[k, side], hidden_send.at[k], hidden_recv.at[k], across
+        )
+
+    def pair_copy(origin):
+        return remote(
+            pair_out.at[origin],
+            pair_in.at[origin],
+            pair_send.at[origin],
+            pair_recv.at[origin],
+            partner,
+        )
+
+    def far_copy(target):
+        return remote(
+            far_out.at[target],
+            far_in.at[chip],
+            far_send.at[target],
+            far_recv.at[chip],
+            {"ep": target * 2 + core},
+        )
+
+    def far_arrival(source):
+        return remote(
+            far_out.at[source],
+            far_in.at[source],
+            far_send.at[source],
+            far_recv.at[source],
+            {"ep": source * 2 + core},
+        )
+
+    token_float = tokens_ref[...].astype(jnp.float32)
+    square_out[0] = jnp.broadcast_to(
+        jnp.sum(token_float * token_float, axis=-1, keepdims=True), (rows, 128)
+    )
+    pl.semaphore_wait(barrier, chips + 1)
+    square_copy(0).start()
+    lane_ids = lax.broadcasted_iota(jnp.int32, (rows, TABLE), 1)
+    table = jnp.zeros((rows, TABLE), jnp.float32)
+    for choice in range(routes_ref.shape[1]):
+        named = routes_ref[:, choice : choice + 1]
+        match = (lane_ids == named) | (lane_ids == named + experts)
+        table = table + jnp.where(match, weights_ref[:, choice : choice + 1], 0.0)
+    coarse = table.astype(jnp.bfloat16).astype(jnp.float32)
+    held[ep, :, width:] = jnp.where(lane_ids < experts, table, table - coarse).astype(jnp.bfloat16)
+    mixture[...] = jnp.zeros_like(mixture)
+    square_copy(0).wait_recv()
+    square = (square_out[0] + square_in[0])[:, :1]
+    gain = norm_gain_ref[:, pl.ds(pl.multiple_of(tp * width, width), width)]
+    held[ep, :, :width] = (
+        tokens_ref[...].astype(jnp.float32) * lax.rsqrt(square / (2 * width) + epsilon) * gain
+    ).astype(jnp.bfloat16)
+
+    gather_copy(chip, 2).start()
+
+    @pl.when(chip > 0)
+    def _():
+        gather_copy(chip, 0).start()
+
+    @pl.when(chip < chips - 1)
+    def _():
+        gather_copy(chip, 1).start()
+
+    def locate(k):
+        origin = exclusive_or(chip, pick(k, masks), chips)
+        lane = pick(k, lanes)
+        return origin, lane
+
+    def first_stage(k):
+        origin, lane = locate(k)
+        is_shared = k == shared_at
+
+        @pl.when(k == 0)
+        def _():
+            loads[0].wait()
+            loads[1].wait()
+
+        @pl.when(is_shared)
+        def _():
+            loads[2].wait()
+            loads[3].wait()
+
+        for index, position in enumerate(relays):
+            distance = index + 1
+
+            @pl.when((k == position) & (chip >= distance))
+            def _(distance=distance):
+                gather_copy(chip - distance, 0).wait_recv()
+                gather_copy(chip - distance, 2).start()
+
+                @pl.when(chip < chips - 1)
+                def _():
+                    gather_copy(chip - distance, 1).start()
+
+            @pl.when((k == position) & (chip + distance < chips))
+            def _(distance=distance):
+                gather_copy(chip + distance, 1).wait_recv()
+                gather_copy(chip + distance, 2).start()
+
+                @pl.when(chip > 0)
+                def _():
+                    gather_copy(chip + distance, 0).start()
+
+        @pl.when((lane != core) & (k != shared_at))
+        def _():
+            pair_gather_arrival(origin).wait_recv()
+
+        block = jnp.where(is_shared, ep, origin * 2 + lane)
+        kind = jnp.where(is_shared, 1, 0)
+        source = held[block, :, :width]
+        away = pl.ds(pl.multiple_of((1 - tp) * half, half), half)
+        near = pl.ds(pl.multiple_of(tp * half, half), half)
+        for which, matrix in enumerate((gate, up)):
+            part_out[k, which] = jnp.dot(
+                source, matrix[kind, :, away], preferred_element_type=jnp.float32
+            ).astype(jnp.bfloat16)
+        part_copy(k).start()
+        for which, matrix in enumerate((gate, up)):
+            part_own[k, which] = jnp.dot(
+                source, matrix[kind, :, near], preferred_element_type=jnp.float32
+            ).astype(jnp.bfloat16)
+
+    def second_stage(k):
+        part_copy(k).wait_recv()
+        gate_sum = part_own[k, 0].astype(jnp.float32) + part_in[k, 0].astype(jnp.float32)
+        up_sum = part_own[k, 1].astype(jnp.float32) + part_in[k, 1].astype(jnp.float32)
+        hidden[k, tp] = (jax.nn.silu(gate_sum) * up_sum).astype(jnp.bfloat16)
+        hidden_copy(k, tp).start()
+
+    def third_stage(k):
+        origin, lane = locate(k)
+        is_shared = k == shared_at
+
+        @pl.when(k == 0)
+        def _():
+            loads[4].wait()
+            loads[5].wait()
+
+        hidden_copy(k, 1 - tp).wait_recv()
+        block = jnp.where(is_shared, ep, origin * 2 + lane)
+        kind = jnp.where(is_shared, 1, 0)
+        chosen = (lane_ids == ep) | (lane_ids == ep + experts)
+        scale = jnp.sum(
+            jnp.where(chosen, held[block, :, width:].astype(jnp.float32), 0.0),
+            axis=-1,
+            keepdims=True,
+        )
+        tile = width // 4
+
+        def tile_step(i, carry):
+            columns = pl.ds(pl.multiple_of(i * tile, tile), tile)
+            product[:, columns] = jnp.dot(
+                hidden[k, 0], down[kind, :half, columns], preferred_element_type=jnp.float32
+            ) + jnp.dot(
+                hidden[k, 1], down[kind, half:, columns], preferred_element_type=jnp.float32
+            )
+            return carry
+
+        lax.fori_loop(0, 4, tile_step, 0)
+
+        def weighted():
+            return product[...].astype(jnp.bfloat16).astype(jnp.float32) * scale
+
+        @pl.when(is_shared)
+        def _():
+            mixture[...] += product[...]
+
+        @pl.when((k != shared_at) & (lane != core))
+        def _():
+            pair_out[origin] = weighted().astype(jnp.bfloat16)
+            pair_copy(origin).start()
+
+        @pl.when((k != shared_at) & (lane == core))
+        def _():
+            pair_copy(origin).wait_recv()
+
+            @pl.when(origin == chip)
+            def _():
+                mixture[...] += weighted() + pair_in[origin].astype(jnp.float32)
+
+            @pl.when(origin != chip)
+            def _():
+                far_out[origin] = (weighted() + pair_in[origin].astype(jnp.float32)).astype(
+                    jnp.bfloat16
+                )
+                far_copy(origin).start()
+
+    def body(i, carry):
+        @pl.when(i < count)
+        def _():
+            first_stage(i)
+
+        @pl.when((i >= 1) & (i < count + 1))
+        def _():
+            second_stage(i - 1)
+
+        @pl.when(i >= 2)
+        def _():
+            third_stage(i - 2)
+
+        return carry
+
+    lax.fori_loop(0, count + 2, body, 0)
+
+    for shift in range(1, chips):
+        source = lax.rem(chip + shift, chips)
+        far_arrival(source).wait_recv()
+        mixture[...] += far_in[source].astype(jnp.float32)
+
+    mixed = mixture[...]
+    square_out[1] = jnp.broadcast_to(jnp.sum(mixed * mixed, axis=-1, keepdims=True), (rows, 128))
+    square_copy(1).start()
+    square_copy(1).wait_recv()
+    total = (square_out[1] + square_in[1])[:, :1]
+    out_ref[...] = (
+        mixture[...] * lax.rsqrt(total / (2 * width) + epsilon) * out_gain_ref[...]
+    ).astype(jnp.bfloat16)
+
+    square_copy(0).wait_send()
+    square_copy(1).wait_send()
+    for origin in range(chips):
+        gather_copy(origin, 2).wait_send()
+        pair_copy(origin).wait_send()
+
+        @pl.when((chip >= origin) & (chip < chips - 1))
+        def _(origin=origin):
+            gather_copy(origin, 1).wait_send()
+
+        @pl.when((chip <= origin) & (chip > 0))
+        def _(origin=origin):
+            gather_copy(origin, 0).wait_send()
+
+        @pl.when(chip != origin)
+        def _(origin=origin):
+            far_copy(origin).wait_send()
+
+    def drain(k, carry):
+        part_copy(k).wait_send()
+        hidden_copy(k, tp).wait_send()
+        return carry
+
+    lax.fori_loop(0, count, drain, 0)
+
+
+def fused(
+    chips,
+    tokens,
+    routes,
+    route_weights,
+    norm_gain,
+    expert_gate,
+    expert_up,
+    expert_down,
+    shared_gate,
+    shared_up,
+    shared_down,
+    out_gain,
+):
+    rows, width = tokens.shape
+    units = shared_gate.shape[1]
+    half = units // 2
+    count = 2 * chips + 1
+    vmem = pl.BlockSpec(memory_space=pltpu.VMEM)
+    hbm = pl.BlockSpec(memory_space=pl.ANY)
+    bf16, f32 = jnp.bfloat16, jnp.float32
+    dma = pltpu.SemaphoreType.DMA
+    return pl.pallas_call(
+        functools.partial(fused_kernel, chips),
+        out_shape=jax.ShapeDtypeStruct((rows, width), bf16),
+        in_specs=[vmem] * 4 + [hbm] * 6 + [vmem],
+        out_specs=vmem,
+        scratch_shapes=[
+            pltpu.VMEM((2, width, units), bf16),
+            pltpu.VMEM((2, width, units), bf16),
+            pltpu.VMEM((2, units, width), bf16),
+            pltpu.VMEM((2 * chips, rows, width + TABLE), bf16),
+            pltpu.VMEM((count, 2, rows, half), bf16),
+            pltpu.VMEM((count, 2, rows, half), bf16),
+            pltpu.VMEM((count, 2, rows, half), bf16),
+            pltpu.VMEM((count, 2, rows, half), bf16),
+            pltpu.VMEM((rows, width), f32),
+            pltpu.VMEM((chips, rows, width), bf16),
+            pltpu.VMEM((chips, rows, width), bf16),
+            pltpu.VMEM((chips, rows, width), bf16),
+            pltpu.VMEM((chips, rows, width), bf16),
+            pltpu.VMEM((rows, width), f32),
+            pltpu.VMEM((2, rows, 128), f32),
+            pltpu.VMEM((2, rows, 128), f32),
+            dma((6,)),
+            dma((2,)),
+            dma((2,)),
+            dma((chips, 3)),
+            dma((chips,)),
+            dma((chips,)),
+            dma((count,)),
+            dma((count,)),
+            dma((count,)),
+            dma((count,)),
+            dma((chips,)),
+            dma((chips,)),
+            dma((chips,)),
+            dma((chips,)),
+        ],
+        compiler_params=pltpu.CompilerParams(
+            collective_id=0, has_side_effects=True, vmem_limit_bytes=60 * 1024 * 1024
+        ),
+    )(
+        tokens,
+        routes,
+        route_weights,
+        norm_gain.reshape(1, -1),
+        expert_gate,
+        expert_up,
+        expert_down,
+        shared_gate,
+        shared_up,
+        shared_down,
+        out_gain.reshape(1, -1),
+    )
 
 
 def local_product(source, matrix):
@@ -77,8 +553,14 @@
 
 
 def solution(mesh):
+    chips = mesh.shape["ep"] // 2
+    powers = chips >= 2 and chips & (chips - 1) == 0 and mesh.shape["ep"] % 2 == 0
+    if mesh.shape["tp"] == 2 and powers and chips * 4 <= TABLE:
+        body = functools.partial(fused, chips)
+    else:
+        body = per_device
     return jax.shard_map(
-        per_device,
+        body,
         mesh=mesh,
         in_specs=(
             P(("grp", "ep"), "tp"),

time: 294 us -> 115 us (0.39); the launches traced: 289 us -> 115 us
  waiting for transfers between devices: 219 us -> 0 us
  Pallas kernels: 0 us -> 110 us
  matrix products: 34.1 us -> 0 us
  blocking collectives: 17.3 us -> 0 us
  between operations: 13.2 us -> 0.01 us
  other arithmetic: 4.88 us -> 0 us
  local copies, waits for them, and re-layouts: 0.66 us -> 4.7 us
    pallas_call x0 -> x1, Pallas kernels: none -> 110 us  [fused(): pl.pallas_call(functools.partial(fused_kernel, chips), out_shape=jax.Shap...]
    psum x1 -> x0, waiting for transfers between devices: 105 us -> none  [per_device(): lax.psum(local_product(expert_input, up_matrix).astype(jnp.bfloat16), 'tp')]
    all_gather x2 -> x0, waiting for transfers between devices: 64.7 us -> none  [the longest x1 40.9 us: per_device(): expert_input = lax.all_gather(normed_block, 'ep', axis=0, tiled=True)]
    reduce_scatter x1 -> x0, waiting for transfers between devices: 49 us -> none  [per_device(): lax.psum_scatter((column * expert_rows.astype(jnp.float32)).astype(jnp.bf...]
    dot_general x6 -> x0, matrix products: 34.1 us -> none  [local_product(): return jnp.dot(source, matrix, preferred_element_type=jnp.float32)]
    all_gather x1 -> x0, blocking collectives: 13.5 us -> none  [per_device(): table_all = lax.all_gather(weight_table, 'ep', axis=0, tiled=True)]
    unnamed x18 -> x3, local copies, waits for them, and re-layouts: 0.65 us -> 4.7 us
    psum x1 -> x0, blocking collectives: 3.78 us -> none  [per_device(): lax.psum(jnp.sum(mixture * mixture, axis=-1, keepdims=True), 'tp')]
  transfers between devices with their start and end apart: 4 -> 0, of which waited for: 4 -> 0; matrix products, arithmetic and copies ran while one was open for 2% -> 0% of each run, Pallas kernels for 0% -> 0%
where the time goes in v1:
time: 115 us
  Pallas kernels  110 us (96%)
  local copies, waits for them, and re-layouts  4.7 us (4%)
    pallas_call x1, Pallas kernels, fused(): pl.pallas_call(functools.partial(fused_kernel, chips), out_shape=jax.Shap...  110 us
    unnamed x3, local copies, waits for them, and re-layouts  4.7 us

profile of v1, /device:TPU:9, one launch (start us, length us, event | category | flops | bytes accessed | tf_op | source)
XLA Modules:
  0.0 114.9 jit_solution(17054023602282108970)
XLA Ops:
  0.0 1.4 %copy.12.routes_ref = s32[128,4]{1,0:T(8,128)} copy(s32[128,4]{0,1:T(4,128)} %param.12) | data formatting | bytes 4096 | tf_op args[1]
  1.4 1.4 %copy.13.weights_ref = f32[128,4]{1,0:T(8,128)} copy(f32[128,4]{0,1:T(4,128)} %param.13) | data formatting | bytes 4096 | tf_op args[2]
  2.8 110.2 %shard_map.109 = bf16[128,2048]{1,0:T(8,128)(2,1)} custom-call(bf16[128,2048]{1,0:T(8,128)(2,1)} %tokens_ref.1, s32[128,4]{1,0:T(8,128)} %copy.12.routes_ref, f32[128,4]{1,0:T(8,128)} %copy.13.weights_ref, f32[1,4096]{1,0:T(1,128)} %bitcast.2, bf16[1,2048,1024]{2,1,0:T(8,128)(2,1)} %gate_hbm.1, bf16[1,2048,1024]{2,1,0:T(8,128)(2,1)} %up_hbm.1, ...), custom_call_target="tpu_custom_call" | custom-call | tf_op jit(solution)/shard_map/pallas_call | solution.py:430
  113.0 1.9 %copy.15 = bf16[128,2048]{1,0:T(8,128)(2,1)} copy(bf16[128,2048]{1,0:T(8,128)(2,1)} %shard_map.109) | data formatting | bytes 1048576

commit v2 on v1

--- a/solution.py
+++ b/solution.py
@@ -13,13 +13,11 @@
 
 
 def plan(chips):
-    steps = [(0, 0), None, (1, 0)]
-    for mask in range(2, chips):
-        steps += [(mask, 0), (mask, 1)]
-    steps += [(1, 1), (0, 1)]
-    relays = []
-    for distance in range(1, chips):
-        relays.append(next(i for i, s in enumerate(steps) if s is not None and s[0] >= distance))
+    ring = [mask for mask in range(2, chips)]
+    first = [(0, 0), (0, 1), (1, 0)]
+    steps = first + [(mask, 0) for mask in ring] + [(mask, 1) for mask in ring] + [(1, 1), None]
+    relays = [[steps.index((distance, 0)), steps.index((max(distance, 2), 1))] for distance in range(1, chips)]
+    relays[0][1] -= 1
     return steps, relays
 
 
@@ -41,18 +39,23 @@
 
 def fused_kernel(
     chips,
-    tokens_ref,
-    routes_ref,
-    weights_ref,
-    norm_gain_ref,
+    tokens_hbm,
+    routes_hbm,
+    weights_hbm,
+    norm_gain_hbm,
     gate_hbm,
     up_hbm,
     down_hbm,
     shared_gate_hbm,
     shared_up_hbm,
     shared_down_hbm,
+    out_gain_hbm,
+    out_ref,
+    tokens_ref,
+    routes_ref,
+    weights_ref,
+    norm_gain_ref,
     out_gain_ref,
-    out_ref,
     gate,
     up,
     down,
@@ -62,6 +65,7 @@
     part_own,
     hidden,
     product,
+    waiting,
     pair_out,
     pair_in,
     far_out,
@@ -111,10 +115,15 @@
                 (shared_up_hbm, up.at[1]),
                 (down_hbm.at[0], down.at[0]),
                 (shared_down_hbm, down.at[1]),
+                (tokens_hbm, tokens_ref),
+                (routes_hbm, routes_ref),
+                (weights_hbm, weights_ref),
+                (norm_gain_hbm, norm_gain_ref),
+                (out_gain_hbm, out_gain_ref),
             ]
         )
     ]
-    for load in loads:
+    for load in loads[6:] + loads[:2]:
         load.start()
 
     barrier = pltpu.get_barrier_semaphore()
@@ -174,55 +183,69 @@
             partner,
         )
 
-    def far_copy(target):
+    beside, opposite, beyond = (exclusive_or(chip, mask, chips) for mask in (1, 2, 3))
+
+    def far_copy(mask, origin):
+        slot = jnp.where(mask == 2, beyond, chip)
         return remote(
-            far_out.at[target],
-            far_in.at[chip],
-            far_send.at[target],
-            far_recv.at[chip],
-            {"ep": target * 2 + core},
-        )
-
-    def far_arrival(source):
+            far_out.at[origin],
+            far_in.at[slot],
+            far_send.at[origin],
+            far_recv.at[slot],
+            {"ep": jnp.where(mask == 3, beyond, beside) * 2 + core},
+        )
+
+    def far_arrival(slot):
         return remote(
-            far_out.at[source],
-            far_in.at[source],
-            far_send.at[source],
-            far_recv.at[source],
-            {"ep": source * 2 + core},
-        )
-
+            far_out.at[slot],
+            far_in.at[slot],
+            far_send.at[slot],
+            far_recv.at[slot],
+            {"ep": beside * 2 + core},
+        )
+
+    def pack(column):
+        return jnp.transpose(jnp.broadcast_to(column, (rows, 128)))[:8]
+
+    def unpack(row):
+        return jnp.transpose(jnp.broadcast_to(row[:1], (128, rows)))[:, :1]
+
+    for load in loads[6:]:
+        load.wait()
     token_float = tokens_ref[...].astype(jnp.float32)
-    square_out[0] = jnp.broadcast_to(
-        jnp.sum(token_float * token_float, axis=-1, keepdims=True), (rows, 128)
-    )
+    own_square = jnp.sum(token_float * token_float, axis=-1, keepdims=True)
+    square_out[0] = pack(own_square)
     pl.semaphore_wait(barrier, chips + 1)
     square_copy(0).start()
     lane_ids = lax.broadcasted_iota(jnp.int32, (rows, TABLE), 1)
-    table = jnp.zeros((rows, TABLE), jnp.float32)
-    for choice in range(routes_ref.shape[1]):
-        named = routes_ref[:, choice : choice + 1]
-        match = (lane_ids == named) | (lane_ids == named + experts)
-        table = table + jnp.where(match, weights_ref[:, choice : choice + 1], 0.0)
+    expert_ids = lax.broadcasted_iota(jnp.int32, (TABLE, rows), 0)
+    table = jnp.zeros((TABLE, rows), jnp.float32)
+    for choice in range(routes_ref.shape[0]):
+        named = routes_ref[choice : choice + 1, :]
+        match = (expert_ids == named) | (expert_ids == named + experts)
+        table = table + jnp.where(match, weights_ref[choice : choice + 1, :], 0.0)
+    table = jnp.transpose(table)
     coarse = table.astype(jnp.bfloat16).astype(jnp.float32)
     held[ep, :, width:] = jnp.where(lane_ids < experts, table, table - coarse).astype(jnp.bfloat16)
     mixture[...] = jnp.zeros_like(mixture)
     square_copy(0).wait_recv()
-    square = (square_out[0] + square_in[0])[:, :1]
+    square = own_square + unpack(square_in[0])
     gain = norm_gain_ref[:, pl.ds(pl.multiple_of(tp * width, width), width)]
     held[ep, :, :width] = (
         tokens_ref[...].astype(jnp.float32) * lax.rsqrt(square / (2 * width) + epsilon) * gain
     ).astype(jnp.bfloat16)
 
+    def send_outward():
+        @pl.when(chip > 0)
+        def _():
+            gather_copy(chip, 0).start()
+
+        @pl.when(chip < chips - 1)
+        def _():
+            gather_copy(chip, 1).start()
+
     gather_copy(chip, 2).start()
-
-    @pl.when(chip > 0)
-    def _():
-        gather_copy(chip, 0).start()
-
-    @pl.when(chip < chips - 1)
-    def _():
-        gather_copy(chip, 1).start()
+    pl.when(core == 0)(send_outward)
 
     def locate(k):
         origin = exclusive_or(chip, pick(k, masks), chips)
@@ -237,14 +260,17 @@
         def _():
             loads[0].wait()
             loads[1].wait()
+            for load in loads[2:6]:
+                load.start()
 
         @pl.when(is_shared)
         def _():
             loads[2].wait()
             loads[3].wait()
 
-        for index, position in enumerate(relays):
+        for index, positions in enumerate(relays):
             distance = index + 1
+            position = jnp.where(core == 0, positions[0], positions[1])
 
             @pl.when((k == position) & (chip >= distance))
             def _(distance=distance):
@@ -335,46 +361,68 @@
 
         @pl.when((k != shared_at) & (lane == core))
         def _():
+            waiting[...] = weighted()
+
+    def fourth_stage(k):
+        origin, lane = locate(k)
+
+        @pl.when((k != shared_at) & (lane == core))
+        def _():
             pair_copy(origin).wait_recv()
 
             @pl.when(origin == chip)
             def _():
-                mixture[...] += weighted() + pair_in[origin].astype(jnp.float32)
+                mixture[...] += waiting[...] + pair_in[origin].astype(jnp.float32)
+
+            mask = pick(k, masks)
+
+            @pl.when(mask == 3)
+            def _():
+                far_arrival(opposite).wait_recv()
+                waiting[...] += far_in[opposite].astype(jnp.float32)
 
             @pl.when(origin != chip)
             def _():
-                far_out[origin] = (weighted() + pair_in[origin].astype(jnp.float32)).astype(
+                far_out[origin] = (waiting[...] + pair_in[origin].astype(jnp.float32)).astype(
                     jnp.bfloat16
                 )
-                far_copy(origin).start()
+                far_copy(mask, origin).start()
 
     def body(i, carry):
         @pl.when(i < count)
         def _():
             first_stage(i)
 
+        @pl.when(i >= 3)
+        def _():
+            fourth_stage(i - 3)
+
         @pl.when((i >= 1) & (i < count + 1))
         def _():
             second_stage(i - 1)
 
-        @pl.when(i >= 2)
+        @pl.when((i == 2) & (core == 1))
+        def _():
+            send_outward()
+
+        @pl.when((i >= 2) & (i < count + 2))
         def _():
             third_stage(i - 2)
 
         return carry
 
-    lax.fori_loop(0, count + 2, body, 0)
-
-    for shift in range(1, chips):
-        source = lax.rem(chip + shift, chips)
-        far_arrival(source).wait_recv()
-        mixture[...] += far_in[source].astype(jnp.float32)
+    lax.fori_loop(0, count + 3, body, 0)
+
+    far_arrival(beside).wait_recv()
+    far_arrival(beyond).wait_recv()
+    mixture[...] += far_in[beside].astype(jnp.float32) + far_in[beyond].astype(jnp.float32)
 
     mixed = mixture[...]
-    square_out[1] = jnp.broadcast_to(jnp.sum(mixed * mixed, axis=-1, keepdims=True), (rows, 128))
+    own_total = jnp.sum(mixed * mixed, axis=-1, keepdims=True)
+    square_out[1] = pack(own_total)
     square_copy(1).start()
     square_copy(1).wait_recv()
-    total = (square_out[1] + square_in[1])[:, :1]
+    total = own_total + unpack(square_in[1])
     out_ref[...] = (
         mixture[...] * lax.rsqrt(total / (2 * width) + epsilon) * out_gain_ref[...]
     ).astype(jnp.bfloat16)
@@ -395,7 +443,7 @@
 
         @pl.when(chip != origin)
         def _(origin=origin):
-            far_copy(origin).wait_send()
+            far_arrival(origin).wait_send()
 
     def drain(k, carry):
         part_copy(k).wait_send()
@@ -423,6 +471,7 @@
     units = shared_gate.shape[1]
     half = units // 2
     count = 2 * chips + 1
+    choices = routes.shape[1]
     vmem = pl.BlockSpec(memory_space=pltpu.VMEM)
     hbm = pl.BlockSpec(memory_space=pl.ANY)
     bf16, f32 = jnp.bfloat16, jnp.float32
@@ -430,9 +479,14 @@
     return pl.pallas_call(
         functools.partial(fused_kernel, chips),
         out_shape=jax.ShapeDtypeStruct((rows, width), bf16),
-        in_specs=[vmem] * 4 + [hbm] * 6 + [vmem],
+        in_specs=[hbm] * 11,
         out_specs=vmem,
         scratch_shapes=[
+            pltpu.VMEM((rows, width), bf16),
+            pltpu.VMEM((choices, rows), jnp.int32),
+            pltpu.VMEM((choices, rows), f32),
+            pltpu.VMEM((1, norm_gain.shape[0]), f32),
+            pltpu.VMEM((1, width), f32),
             pltpu.VMEM((2, width, units), bf16),
             pltpu.VMEM((2, width, units), bf16),
             pltpu.VMEM((2, units, width), bf16),
@@ -442,14 +496,15 @@
             pltpu.VMEM((count, 2, rows, half), bf16),
             pltpu.VMEM((count, 2, rows, half), bf16),
             pltpu.VMEM((rows, width), f32),
+            pltpu.VMEM((rows, width), f32),
             pltpu.VMEM((chips, rows, width), bf16),
             pltpu.VMEM((chips, rows, width), bf16),
             pltpu.VMEM((chips, rows, width), bf16),
             pltpu.VMEM((chips, rows, width), bf16),
             pltpu.VMEM((rows, width), f32),
-            pltpu.VMEM((2, rows, 128), f32),
-            pltpu.VMEM((2, rows, 128), f32),
-            dma((6,)),
+            pltpu.VMEM((2, 8, rows), f32),
+            pltpu.VMEM((2, 8, rows), f32),
+            dma((11,)),
             dma((2,)),
             dma((2,)),
             dma((chips, 3)),
@@ -469,8 +524,8 @@
         ),
     )(
         tokens,
-        routes,
-        route_weights,
+        routes.T,
+        route_weights.T,
         norm_gain.reshape(1, -1),
         expert_gate,
         expert_up,
@@ -554,8 +609,7 @@
 
 def solution(mesh):
     chips = mesh.shape["ep"] // 2
-    powers = chips >= 2 and chips & (chips - 1) == 0 and mesh.shape["ep"] % 2 == 0
-    if mesh.shape["tp"] == 2 and powers and chips * 4 <= TABLE:
+    if mesh.shape["tp"] == 2 and mesh.shape["ep"] == 8:
         body = functools.partial(fused, chips)
     else:
         body = per_device

time: 115 us -> 100 us (0.87)
  Pallas kernels: 110 us -> 97.1 us
  local copies, waits for them, and re-layouts: 4.7 us -> 1.88 us
    pallas_call x1, Pallas kernels: 110 us -> 97.1 us  [fused(): pl.pallas_call(functools.partial(fused_kernel, chips), out_shape=jax.Shap...]
    unnamed x3 -> x1, local copies, waits for them, and re-layouts: 4.7 us -> 1.88 us
where the time goes in v2:
time: 100 us; the launch traced here: 99 us
  Pallas kernels  97.1 us (97%)
  local copies, waits for them, and re-layouts  1.88 us (2%)
    pallas_call x1, Pallas kernels, fused(): pl.pallas_call(functools.partial(fused_kernel, chips), out_shape=jax.Shap...  97.1 us

profile of v2, /device:TPU:9, one launch (start us, length us, event | category | flops | bytes accessed | tf_op | source)
XLA Modules:
  0.0 99.0 jit_solution(1915914714969900584)
XLA Ops:
  0.0 97.1 %shard_map.109 = bf16[128,2048]{1,0:T(8,128)(2,1)} custom-call(bf16[128,2048]{1,0:T(8,128)(2,1)} %tokens_hbm.1, s32[4,128]{1,0:T(4,128)} %bitcast.6, f32[4,128]{1,0:T(4,128)} %bitcast.7, f32[1,4096]{1,0:T(1,128)} %bitcast.4, bf16[1,2048,1024]{2,1,0:T(8,128)(2,1)} %gate_hbm.1, bf16[1,2048,1024]{2,1,0:T(8,128)(2,1)} %up_hbm.1, ...), custom_call_target="tpu_custom_call" | custom-call | tf_op jit(solution)/shard_map/pallas_call | solution.py:479
  97.1 1.9 %copy.13 = bf16[128,2048]{1,0:T(8,128)(2,1)} copy(bf16[128,2048]{1,0:T(8,128)(2,1)} %shard_map.109) | data formatting | bytes 1048576

commit v3 on v2

--- a/solution.py
+++ b/solution.py
@@ -166,8 +166,14 @@
         slot = held.at[origin * 2 + other_core]
         return remote(slot, slot, gather_send.at[origin, 2], pair_gather_recv.at[origin], partner)
 
-    def part_copy(k):
-        return remote(part_out.at[k], part_in.at[k], part_send.at[k], part_recv.at[k], across)
+    def part_copy(k, which):
+        return remote(
+            part_out.at[k, which],
+            part_in.at[k, which],
+            part_send.at[k, which],
+            part_recv.at[k, which],
+            across,
+        )
 
     def hidden_copy(k, side):
         return remote(
@@ -303,14 +309,15 @@
             part_out[k, which] = jnp.dot(
                 source, matrix[kind, :, away], preferred_element_type=jnp.float32
             ).astype(jnp.bfloat16)
-        part_copy(k).start()
+            part_copy(k, which).start()
         for which, matrix in enumerate((gate, up)):
             part_own[k, which] = jnp.dot(
                 source, matrix[kind, :, near], preferred_element_type=jnp.float32
             ).astype(jnp.bfloat16)
 
     def second_stage(k):
-        part_copy(k).wait_recv()
+        part_copy(k, 0).wait_recv()
+        part_copy(k, 1).wait_recv()
         gate_sum = part_own[k, 0].astype(jnp.float32) + part_in[k, 0].astype(jnp.float32)
         up_sum = part_own[k, 1].astype(jnp.float32) + part_in[k, 1].astype(jnp.float32)
         hidden[k, tp] = (jax.nn.silu(gate_sum) * up_sum).astype(jnp.bfloat16)
@@ -446,7 +453,8 @@
             far_arrival(origin).wait_send()
 
     def drain(k, carry):
-        part_copy(k).wait_send()
+        part_copy(k, 0).wait_send()
+        part_copy(k, 1).wait_send()
         hidden_copy(k, tp).wait_send()
         return carry
 
@@ -510,8 +518,8 @@
             dma((chips, 3)),
             dma((chips,)),
             dma((chips,)),
-            dma((count,)),
-            dma((count,)),
+            dma((count, 2)),
+            dma((count, 2)),
             dma((count,)),
             dma((count,)),
             dma((chips,)),

time: 100 us -> 99.6 us (level)
  no operation moved by 1% of the time
where the time goes in v3:
time: 99.6 us; the launch traced here: 98.5 us
  Pallas kernels  96.6 us (97%)
  local copies, waits for them, and re-layouts  1.88 us (2%)
    pallas_call x1, Pallas kernels, fused(): pl.pallas_call(functools.partial(fused_kernel, chips), out_shape=jax.Shap...  96.6 us

profile of v3, /device:TPU:9, one launch (start us, length us, event | category | flops | bytes accessed | tf_op | source)
XLA Modules:
  0.0 98.5 jit_solution(1353192717544122671)
XLA Ops:
  0.0 96.6 %shard_map.109 = bf16[128,2048]{1,0:T(8,128)(2,1)} custom-call(bf16[128,2048]{1,0:T(8,128)(2,1)} %tokens_hbm.1, s32[4,128]{1,0:T(4,128)} %bitcast.6, f32[4,128]{1,0:T(4,128)} %bitcast.7, f32[1,4096]{1,0:T(1,128)} %bitcast.4, bf16[1,2048,1024]{2,1,0:T(8,128)(2,1)} %gate_hbm.1, bf16[1,2048,1024]{2,1,0:T(8,128)(2,1)} %up_hbm.1, ...), custom_call_target="tpu_custom_call" | custom-call | tf_op jit(solution)/shard_map/pallas_call | solution.py:487
  96.6 1.9 %copy.13 = bf16[128,2048]{1,0:T(8,128)(2,1)} copy(bf16[128,2048]{1,0:T(8,128)(2,1)} %shard_map.109) | data formatting | bytes 1048576
